TPU v7x, 32 devices: a whole 2x2x4 slice. The times are simulated.
32 devices in a mesh: sp: 8 (over z, x), tp: 4 (over y, core).
Axes of the slice: x: 2, y: 2, z: 4, core: 2. Of those that a mesh axis runs over, the one named last changes fastest.
Arguments:
- tokens: bfloat16 [1024, 2048], P('sp', 'tp'), may hold values from -6 to 6
- norm_gain: float32 [2048], replicated, may hold values from 0.1 to 1.9
- da_query: bfloat16 [2048, 1024], P(None, 'tp'), as said below
- da_key: bfloat16 [2048, 1024], P(None, 'tp'), may hold values from -0.125 to 0.125
- da_value: bfloat16 [2048, 1024], P(None, 'tp'), may hold values from -0.125 to 0.125
- mix_lambda: float32 [8], P('tp'), may hold values from 0.3 to 0.8
- attn_gain: float32 [128], replicated, may hold values from 0.1 to 1.9
- rec_query: bfloat16 [2048, 1024], P(None, 'tp'), may hold values from -0.125 to 0.125
- rec_forget_fwd: bfloat16 [2048, 1024], P(None, 'tp'), may hold values from -0.375 to 0.375
- rec_forget_bwd: bfloat16 [2048, 1024], P(None, 'tp'), may hold values from -0.375 to 0.375
- rec_value: bfloat16 [2048, 1024], P(None, 'tp'), may hold values from -0.125 to 0.125
- gate_gap: float32 [2, 1024], P(None, 'tp'), may hold values from 0.0009765625 to 0.12
- extra_decay: float32 [2, 1024, 8], P(None, 'sp', 'tp'), may hold values from -0.7 to 0
- init_state: float32 [2, 8, 128, 128], P(None, 'tp'), may hold values from -1.5 to 1.5
- rec_gain: float32 [128], replicated, may hold values from 0.1 to 1.9
- out_attn: bfloat16 [1024, 2048], P('tp'), may hold values from -0.125 to 0.125
- out_rec: bfloat16 [1024, 2048], P('tp'), may hold values from -0.125 to 0.125
Outputs:
- mixed: bfloat16 [1024, 2048], P(('sp', 'tp'))
Inputs may be any that keep to these rules, and one draw needn't show every extreme that they name: `da_query`: entries lie within -240 / sqrt(2048) and 240 / sqrt(2048).
All inputs are finite; a program needn't handle non-finite values.
Results may differ from a plain program's by a relative error of at most 0.014.
The roundings to bfloat16 on the way count: a program that leaves them out, or rounds other values in their place, can miss the bound.
Values may be sent and summed in bfloat16 or wider, within the bound.
A program may use at most 128 MiB of HBM per device.

v0:
```python
import jax
import jax.numpy as jnp
from jax import lax
from jax.sharding import PartitionSpec as P

D = 2048
QK_DIM = 64
DA_VAL = 128
HG_KEY = 128
HG_VAL = 128
SPAN = 64


EPSILON = 1e-06
EXACT_PRECISION = lax.Precision.HIGHEST


def prefix(value, axis, join, neutral, backward):
    count = lax.axis_size(axis)
    place = lax.axis_index(axis)
    ahead = count - 1 - place if backward else place
    gathered = jax.tree.map(
        lambda a, kind: lax.all_gather(a.astype(kind), axis), value, (jnp.bfloat16, jnp.bfloat16)
    )
    state = jax.tree.map(lambda a, e: jnp.zeros_like(a) + jnp.asarray(e, a.dtype), value, neutral)

    def one(lap, state):
        source = count - 1 - lap if backward else lap
        return join(
            state,
            jax.tree.map(
                lambda a, own: lax.dynamic_index_in_dim(a, source, 0, False).astype(own.dtype),
                gathered,
                value,
            ),
        )

    return lax.fori_loop(0, ahead, one, state)


def block_scan(query, key_in, values, log_decay, initial):
    length = query.shape[0]
    count = length // SPAN

    def split(array):
        return array.reshape((count, SPAN) + array.shape[1:])

    lower = jnp.tril(jnp.ones((SPAN, SPAN), jnp.float32))

    def block_one_step(carried_state, inputs):
        query_tile, key_tile, value_tile, g_block = inputs
        cumulative_decay = jnp.cumsum(g_block, axis=0)
        relative = cumulative_decay[:, None] - cumulative_decay[None, :]
        relative = jnp.where(lower[:, :, None, None] > 0, relative, -jnp.inf)
        score_matrix = jnp.einsum(
            "ihk,ijhk,jhk->hij", query_tile, jnp.exp(relative), key_tile, precision=EXACT_PRECISION
        )
        output_rows = jnp.einsum(
            "ujg,jga->uja",
            query_tile * jnp.exp(cumulative_decay),
            carried_state,
            precision=EXACT_PRECISION,
        ) + jnp.einsum("ots,sok->tok", score_matrix, value_tile, precision=EXACT_PRECISION)
        ending_state = cumulative_decay[-1]
        carried_state = jnp.exp(ending_state)[..., None] * carried_state + jnp.einsum(
            "zds,zdx->dsx",
            key_tile * jnp.exp(ending_state[None] - cumulative_decay),
            value_tile,
            precision=EXACT_PRECISION,
        )
        return (carried_state, output_rows)

    carried_state, output_rows = lax.scan(
        block_one_step, initial, (split(query), split(key_in), split(values), split(log_decay))
    )
    return (output_rows.reshape((length,) + output_rows.shape[2:]), carried_state)


def combine_states(earlier, later):
    return (earlier[0] + later[0], jnp.exp(later[0])[..., None] * earlier[1] + later[1])


def local(
    tokens,
    norm_gain,
    da_query,
    da_key,
    da_value,
    mix_lambda,
    attn_gain,
    rec_query,
    rec_forget_fwd,
    rec_forget_bwd,
    rec_value,
    gate_gap,
    extra_decay,
    init_state,
    rec_gain,
    out_attn,
    out_rec,
):
    row_count = tokens.shape[0]
    weight_list = (da_query, da_key, da_value, rec_query, rec_forget_fwd, rec_forget_bwd, rec_value)
    values = lax.all_gather(tokens, "tp", axis=1, tiled=True).astype(jnp.float32)
    scaled = (values * norm_gain).astype(jnp.bfloat16)
    updated = tuple(
        (jnp.dot(scaled, weight, preferred_element_type=jnp.float32) for weight in weight_list)
    )
    squares = jnp.sum(values * values, axis=1)
    inv_rms = lax.rsqrt(squares / D + EPSILON)[:, None]
    query_att, key_att, value_att, query_rec, forget_fwd, forget_bwd, value_rec = tuple(
        ((total_now * inv_rms).astype(jnp.bfloat16) for total_now in updated)
    )
    head_count = mix_lambda.shape[0]
    queries = query_att.reshape(row_count, head_count, 2, QK_DIM)
    rec_heads = query_rec.shape[1] // HG_KEY

    def heads(array, width):
        return array.astype(jnp.float32).reshape(row_count, rec_heads, width)

    start_state = (
        jnp.full((head_count, 2, row_count), -jnp.inf, jnp.float32),
        jnp.zeros((head_count, 2, row_count), jnp.float32),
        jnp.zeros((head_count, 2, row_count, DA_VAL), jnp.float32),
    )
    running = start_state
    key_piece = lax.all_gather(key_att, "sp", axis=0, tiled=True)
    value_piece = lax.all_gather(value_att, "sp", axis=0, tiled=True)
    length = key_piece.shape[0]
    step_rows = max((candidate for candidate in range(1, 2049) if length % candidate == 0))
    key_blocks = key_piece.reshape(length // step_rows, step_rows, head_count, 2, QK_DIM)
    value_blocks = value_piece.reshape(length // step_rows, step_rows, head_count, DA_VAL)

    def absorb_one_step(carried_state, inputs):
        maxima, denoms, numerator = carried_state
        key_block, value_block = inputs
        score_matrix = jnp.einsum(
            "qhmd,khmd->hmqk", queries, key_block, preferred_element_type=jnp.float32
        ) * QK_DIM ** (-0.5)
        new_maxima = jnp.maximum(maxima, jnp.max(score_matrix, axis=3))
        factor = jnp.exp(maxima - new_maxima)
        unnorm = jnp.exp(score_matrix - new_maxima[..., None])
        denoms = denoms * factor + jnp.sum(unnorm, axis=3)
        numerator = numerator * factor[..., None] + jnp.einsum(
            "hmqk,khv->hmqv",
            unnorm.astype(jnp.bfloat16),
            value_block,
            preferred_element_type=jnp.float32,
        )
        return ((new_maxima, denoms, numerator), None)

    running, unused = lax.scan(absorb_one_step, running, (key_blocks, value_blocks))
    maxima, denoms, numerator = running
    ratio = numerator / denoms[..., None]
    diff = ratio[:, 0] - mix_lambda[:, None, None] * ratio[:, 1]
    normed = diff * lax.rsqrt(jnp.mean(diff * diff, axis=-1, keepdims=True) + EPSILON) * attn_gain
    attn_out = (
        jnp.transpose(normed, (1, 0, 2))
        .reshape(row_count, head_count * DA_VAL)
        .astype(jnp.bfloat16)
    )
    rec_q = jax.nn.silu(heads(query_rec, HG_KEY)) * HG_KEY ** (-0.5)
    values_rec = heads(value_rec, HG_VAL)
    zero_state = jnp.zeros((rec_heads, HG_KEY, HG_VAL), jnp.float32)
    identity = (jnp.zeros((rec_heads, HG_KEY), jnp.float32), zero_state)

    def prepare(forget, direction):
        gap = gate_gap[direction].reshape(rec_heads, HG_KEY)
        key_in = gap * jax.nn.sigmoid(-heads(forget, HG_KEY))
        log_decay = jnp.log1p(-key_in) + extra_decay[direction][:, :, None]
        return (key_in, log_decay)

    def finish(ordered_query, local_out, ordered_decay, incoming, start_state):
        entering_state = jnp.exp(incoming[0])[..., None] * start_state + incoming[1]
        cumulative_decay = jnp.cumsum(ordered_decay, axis=0)
        return local_out + jnp.einsum(
            "ibe,bef->ibf",
            ordered_query * jnp.exp(cumulative_decay),
            entering_state,
            precision=EXACT_PRECISION,
        )

    key_fwd, decay_fwd = prepare(forget_fwd, 0)
    local_fwd, ending_fwd = block_scan(rec_q, key_fwd, values_rec, decay_fwd, zero_state)
    incoming_fwd = prefix(
        (jnp.sum(decay_fwd, axis=0), ending_fwd), "sp", combine_states, identity, False
    )
    out_fwd = finish(rec_q, local_fwd, decay_fwd, incoming_fwd, init_state[0])
    key_bwd, decay_bwd = prepare(forget_bwd, 1)
    reversed_q = rec_q[::-1]
    reversed_decay = decay_bwd[::-1]
    local_bwd, ending_bwd = block_scan(
        reversed_q, key_bwd[::-1], values_rec[::-1], reversed_decay, zero_state
    )
    incoming_bwd = prefix(
        (jnp.sum(decay_bwd, axis=0), ending_bwd), "sp", combine_states, identity, True
    )
    out_bwd = finish(reversed_q, local_bwd, reversed_decay, incoming_bwd, init_state[1])[::-1]
    rec_sum = out_fwd + out_bwd
    rec_normed = (
        rec_sum
        * lax.rsqrt(jnp.mean(rec_sum * rec_sum, axis=-1, keepdims=True) + EPSILON)
        * rec_gain
    )
    rec_out = rec_normed.reshape(row_count, rec_heads * HG_VAL).astype(jnp.bfloat16)
    attn_rows, rec_rows = (
        lax.all_to_all(attn_out, "tp", split_axis=0, concat_axis=1, tiled=True),
        lax.all_to_all(rec_out, "tp", split_axis=0, concat_axis=1, tiled=True),
    )
    part = attn_rows
    mixed = jnp.dot(
        part, lax.all_gather(out_attn, "tp", axis=0, tiled=True), preferred_element_type=jnp.float32
    )
    part = rec_rows
    mixed = mixed + jnp.dot(
        part, lax.all_gather(out_rec, "tp", axis=0, tiled=True), preferred_element_type=jnp.float32
    )
    return mixed.astype(jnp.bfloat16)


def solution(mesh):
    placed = (
        P("sp", "tp"),
        P(),
        P(None, "tp"),
        P(None, "tp"),
        P(None, "tp"),
        P("tp"),
        P(),
        P(None, "tp"),
        P(None, "tp"),
        P(None, "tp"),
        P(None, "tp"),
        P(None, "tp"),
        P(None, "sp", "tp"),
        P(None, "tp", None, None),
        P(),
        P("tp", None),
        P("tp", None),
    )
    return jax.shard_map(
        local, mesh=mesh, in_specs=placed, out_specs=P(("sp", "tp"), None), check_vma=False
    )
```

profile of v0, /device:TPU:0, one launch (start us, length us, event | category | flops | bytes accessed | tf_op | source)
XLA Modules:
  0.0 277.9 jit_solution(16707672340335798208)
XLA Ops:
  6.5 0.7 all-gather.5.cloned.1.call-update
  7.3 8.9 %all_gather.35 = bf16[128,2048]{1,0:T(8,128)(2,1)S(1)} all-gather(bf16[128,512]{1,0:T(8,128)(2,1)} %param.25), channel_id=1, replica_groups=mesh['sp'=8,'tp'=4] {'tp'}, dimensions={1}, use_global_device_ids=true | all-gather | bytes 655360 | tf_op jit(solution)/shard_map/all_gather | solution.py:104
  16.2 0.2 fusion.69
  16.4 1.6 fusion.53
  18.0 31.9 %all_gather.37 = bf16[1024,256]{1,0:T(8,128)(2,1)S(1)} all-gather(bf16[128,256]{1,0:T(8,128)(2,1)S(1)} %fusion.53), channel_id=1, replica_groups=mesh['sp'=8,'tp'=4] {'sp'}, dimensions={0}, use_global_device_ids=true | all-gather | bytes 589824 | tf_op jit(solution)/shard_map/all_gather | solution.py:128
  49.9 1.0 copy.97
  50.9 0.3 fusion.51
  51.3 1.5 fusion.52
  52.8 31.2 %all_gather.36 = bf16[1024,256]{1,0:T(8,128)(2,1)S(1)} all-gather(bf16[128,256]{1,0:T(8,128)(2,1)S(1)} %fusion.52), channel_id=1, replica_groups=mesh['sp'=8,'tp'=4] {'sp'}, dimensions={0}, use_global_device_ids=true | all-gather | bytes 589824 | tf_op jit(solution)/shard_map/all_gather | solution.py:127
  84.0 0.2 copy.67
  84.3 0.6 multiply_reduce_fusion
  84.8 0.5 fusion.45
  85.4 1.7 fusion.47
  87.4 0.7 convert_element_type.144
  88.1 3.3 %all-to-all-start = ((bf16[4,32,256]{2,1,0:T(8,128)(2,1)}), bf16[4,32,256]{2,1,0:T(8,128)(2,1)S(1)}, u32[]{:S(2)}, u32[]{:S(2)}) async-start(bf16[4,32,256]{2,1,0:T(8,128)(2,1)} %convert_element_type.144), calls=%async_computation | async-start | bytes 131072 | tf_op jit(solution)/shard_map/all_to_all | solution.py:207
  91.4 0.2 all-gather.7.cloned.1.call-start
  91.6 0.5 all-gather.7.cloned.1.call-update
  92.2 0.3 fusion.62
  92.6 1.5 fusion.60
  94.4 0.2 add.202
  94.6 0.4 fusion.73
  95.1 0.2 log-plus-one_add_fusion
  95.6 0.1 fusion.108
  95.7 0.1 divide_multiply_fusion
  96.1 0.2 add.193
  96.3 1.6 fusion.74
  98.0 0.4 log-plus-one_add_fusion.1
  98.4 27.3 %while.60 = (s32[]{:T(128)}, f32[2,128,128]{2,1,0:T(8,128)S(1)}, f32[2,64,2,128]{3,1,0,2:T(8,128)S(1)}, f32[2,64,2,128]{3,2,1,0:T(2,128)S(1)}, f32[2,64,2,128]{3...) while((s32[]{:T(128)}, f32[2,128,128]{2,1,0:T(8,128)S(1)}, ...), condition=%wide.region_6.7_spmd.clone, body=%wide.region_4.6_spmd.clone.sunk | while | flops 79884288 | bytes 10336384 | solution.py:73
  98.6 0.2 convolution_bitcast_fusion.8
  98.9 0.4 convolution_add_fusion.6
  99.3 5.9 %multiply_bitcast_fusion.4 = f32[64,2,128,64]{2,1,0,3:T(2,128)S(1)} fusion(pred[64,64]{1,0:T(8,128)(4,1)S(1)} %select_compare_fusion.4, f32[64,2,128]{2,1,0:T(2,128)S(1)} %get-tuple-element.582, f32[64,2,128]{2,1,0:T(2,128)S(1)} %fusion.159), kind=kLoop, calls=%fused_computation.12.clone.1 | loop fusion | flops 3145728 | bytes 4329472 | tf_op jit(solution)/shard_map/while/body/eval_jaxpr/ihk,ijhk,jhk->hij/dot_general | solution.py:55
  105.2 6.6 %fusion.161 = f32[2,64,1,64]{3,2,1,0:T(1,128)S(1)} fusion(f32[64,2,128,64]{2,1,0,3:T(2,128)S(1)} %multiply_bitcast_fusion.4, f32[64,2,128,1]{2,1,0,3:T(2,128)S(1)} %get-tuple-element.583), kind=kOutput, calls=%fused_computation.10.clone.1 | convolution fusion | flops 12582912 | bytes 4292608 | tf_op jit(solution)/shard_map/while/body/eval_jaxpr/ihk,ijhk,jhk->hij/dot_general | solution.py:55
  111.8 0.2 fusion.162
  112.2 0.2 convolution_bitcast_fusion.8
  112.5 0.4 convolution_add_fusion.6
  112.9 5.9 %multiply_bitcast_fusion.4 = f32[64,2,128,64]{2,1,0,3:T(2,128)S(1)} fusion(pred[64,64]{1,0:T(8,128)(4,1)S(1)} %select_compare_fusion.4, f32[64,2,128]{2,1,0:T(2,128)S(1)} %get-tuple-element.582, f32[64,2,128]{2,1,0:T(2,128)S(1)} %fusion.159), kind=kLoop, calls=%fused_computation.12.clone.1 | loop fusion | flops 3145728 | bytes 4329472 | tf_op jit(solution)/shard_map/while/body/eval_jaxpr/ihk,ijhk,jhk->hij/dot_general | solution.py:55
  118.9 6.6 %fusion.161 = f32[2,64,1,64]{3,2,1,0:T(1,128)S(1)} fusion(f32[64,2,128,64]{2,1,0,3:T(2,128)S(1)} %multiply_bitcast_fusion.4, f32[64,2,128,1]{2,1,0,3:T(2,128)S(1)} %get-tuple-element.583), kind=kOutput, calls=%fused_computation.10.clone.1 | convolution fusion | flops 12582912 | bytes 4292608 | tf_op jit(solution)/shard_map/while/body/eval_jaxpr/ihk,ijhk,jhk->hij/dot_general | solution.py:55
  125.5 0.2 fusion.162
  125.7 0.1 exponential_multiply_fusion.2
  125.9 27.6 %while.61 = (s32[]{:T(128)}, f32[2,128,128]{2,1,0:T(8,128)S(1)}, f32[2,64,2,128]{3,1,0,2:T(8,128)S(1)}, f32[2,64,2,128]{3,2,1,0:T(2,128)S(1)}, f32[2,64,2,128]{3...) while((s32[]{:T(128)}, f32[2,128,128]{2,1,0:T(8,128)S(1)}, ...), condition=%wide.region_13.14_spmd.clone, body=%wide.region_11.13_spmd.clone.sunk | while | flops 79884288 | bytes 10206336 | solution.py:73
  126.3 0.2 convolution_bitcast_fusion.9
  126.6 0.4 convolution_add_fusion.7
  127.0 5.9 %multiply_bitcast_fusion.5 = f32[64,2,128,64]{2,1,0,3:T(2,128)S(1)} fusion(pred[64,64]{1,0:T(8,128)(4,1)S(1)} %select_compare_fusion.5, f32[64,2,128]{2,1,0:T(2,128)S(1)} %get-tuple-element.593, f32[64,2,128]{2,1,0:T(2,128)S(1)} %fusion.172), kind=kLoop, calls=%fused_computation.42.clone.1 | loop fusion | flops 3145728 | bytes 4329472 | tf_op jit(solution)/shard_map/while/body/eval_jaxpr/ihk,ijhk,jhk->hij/dot_general | solution.py:55
  132.9 6.6 %fusion.174 = f32[2,64,1,64]{3,2,1,0:T(1,128)S(1)} fusion(f32[64,2,128,64]{2,1,0,3:T(2,128)S(1)} %multiply_bitcast_fusion.5, f32[64,2,128,1]{2,1,0,3:T(2,128)S(1)} %dynamic-slice_bitcast_fusion.9), kind=kOutput, calls=%fused_computation.40.clone.1 | convolution fusion | flops 12582912 | bytes 4292608 | tf_op jit(solution)/shard_map/while/body/eval_jaxpr/ihk,ijhk,jhk->hij/dot_general | solution.py:55
  139.5 0.2 fusion.175
  140.0 0.2 convolution_bitcast_fusion.9
  140.2 0.4 convolution_add_fusion.7
  140.7 5.9 %multiply_bitcast_fusion.5 = f32[64,2,128,64]{2,1,0,3:T(2,128)S(1)} fusion(pred[64,64]{1,0:T(8,128)(4,1)S(1)} %select_compare_fusion.5, f32[64,2,128]{2,1,0:T(2,128)S(1)} %get-tuple-element.593, f32[64,2,128]{2,1,0:T(2,128)S(1)} %fusion.172), kind=kLoop, calls=%fused_computation.42.clone.1 | loop fusion | flops 3145728 | bytes 4329472 | tf_op jit(solution)/shard_map/while/body/eval_jaxpr/ihk,ijhk,jhk->hij/dot_general | solution.py:55
  146.6 6.6 %fusion.174 = f32[2,64,1,64]{3,2,1,0:T(1,128)S(1)} fusion(f32[64,2,128,64]{2,1,0,3:T(2,128)S(1)} %multiply_bitcast_fusion.5, f32[64,2,128,1]{2,1,0,3:T(2,128)S(1)} %dynamic-slice_bitcast_fusion.9), kind=kOutput, calls=%fused_computation.40.clone.1 | convolution fusion | flops 12582912 | bytes 4292608 | tf_op jit(solution)/shard_map/while/body/eval_jaxpr/ihk,ijhk,jhk->hij/dot_general | solution.py:55
  153.2 0.2 fusion.175
  153.7 20.6 %all_gather.42 = bf16[8,2,128]{2,1,0:T(2,128)(2,1)S(1)} all-gather(bf16[1,2,128]{2,1,0:T(2,128)(2,1)S(1)} %bitcast.287), channel_id=1, replica_groups=mesh['sp'=8,'tp'=4] {'sp'}, dimensions={0}, use_global_device_ids=true | all-gather | bytes 4608 | tf_op jit(solution)/shard_map/all_gather | solution.py:23
  174.3 31.3 %all-gather.1 = bf16[16,128,128]{2,1,0:T(8,128)(2,1)S(1)} all-gather(bf16[2,128,128]{2,1,0:T(8,128)(2,1)S(1)} %convert_element_type.158), channel_id=3, replica_groups=mesh['sp'=8,'tp'=4] {'sp'}, dimensions={0}, use_global_device_ids=true | all-gather | bytes 589824 | tf_op jit(solution)/shard_map/all_gather | solution.py:23
  205.6 1.2 while.59
  206.8 0.5 fusion.50
  207.3 0.2 rev.19
  207.6 16.3 %all_gather.39 = bf16[8,2,128]{2,1,0:T(2,128)(2,1)S(1)} all-gather(bf16[1,2,128]{2,1,0:T(2,128)(2,1)S(1)} %bitcast.286), channel_id=1, replica_groups=mesh['sp'=8,'tp'=4] {'sp'}, dimensions={0}, use_global_device_ids=true | all-gather | bytes 4608 | tf_op jit(solution)/shard_map/all_gather | solution.py:23
  223.9 31.2 %all-gather = bf16[16,128,128]{2,1,0:T(8,128)(2,1)S(1)} all-gather(bf16[2,128,128]{2,1,0:T(8,128)(2,1)S(1)} %convert_element_type.153), channel_id=2, replica_groups=mesh['sp'=8,'tp'=4] {'sp'}, dimensions={0}, use_global_device_ids=true | all-gather | bytes 589824 | tf_op jit(solution)/shard_map/all_gather | solution.py:23
  255.1 0.3 exponential_multiply_fusion.3
  255.4 0.5 multiply_reduce_fusion.1
  256.2 0.7 convert_element_type.160
  256.8 3.4 %all-to-all-start.1 = ((bf16[4,32,256]{2,1,0:T(8,128)(2,1)}), bf16[4,32,256]{2,1,0:T(8,128)(2,1)S(1)}, u32[]{:S(2)}, u32[]{:S(2)}) async-start(bf16[4,32,256]{2,1,0:T(8,128)(2,1)} %convert_element_type.160), calls=%async_computation.1 | async-start | bytes 131072 | tf_op jit(solution)/shard_map/all_to_all | solution.py:208
  260.2 4.1 %all-to-all-done.1 = bf16[4,32,256]{2,1,0:T(8,128)(2,1)S(1)} async-done(((bf16[4,32,256]{2,1,0:T(8,128)(2,1)}), bf16[4,32,256]{2,1,0:T(8,128)(2,1)S(1)}, u32[]{:S(2)}, u32[]{:S(2)}) %all-to-all-start.1) | async-done | bytes 65568 | tf_op jit(solution)/shard_map/all_to_all | solution.py:208
  264.3 3.0 %fusion.109 = f32[32,2048]{1,0:T(8,128)S(1)} fusion(bf16[32,1024]{1,0:T(8,128)(2,1)S(1)} %bitcast.273, bf16[1024,2048]{1,0:T(8,128)(2,1)} %all-gather.5.cloned.1.call-done), kind=kOutput, calls=%fused_computation.170 | convolution fusion | flops 134217728 | bytes 4521984 | tf_op jit(solution)/shard_map/dot_general | solution.py:211
  267.4 3.7 %fusion.44 = bf16[32,2048]{1,0:T(8,128)(2,1)} fusion(f32[32,2048]{1,0:T(8,128)S(1)} %fusion.109, bf16[32,1024]{1,0:T(8,128)(2,1)S(1)} %bitcast.274, bf16[1024,2048]{1,0:T(8,128)(2,1)} %all-gather.7.cloned.1.call-done), kind=kOutput, calls=%fused_computation.75 | convolution fusion | flops 134348800 | bytes 4653056 | tf_op jit(solution)/shard_map/dot_general | solution.py:215
  (104 shorter events, 3.8 us)
Async XLA Ops:
  6.5 88.1 %copy-start = (bf16[2048,256]{1,0:T(8,128)(2,1)S(1)}, bf16[2048,256]{1,0:T(8,128)(2,1)}, u32[]{:S(2)}) copy-start(bf16[2048,256]{1,0:T(8,128)(2,1)} %param.34) | copy-start | bytes 3145732
  6.5 44.3 %copy-start.4 = (f32[2048]{0:T(1024)S(1)}, f32[2048]{0:T(1024)}, u32[]{:S(2)}) copy-start(f32[2048]{0:T(1024)} %param.26) | copy-start | bytes 24580
  6.5 44.3 %copy-start.1 = (bf16[2048,256]{1,0:T(8,128)(2,1)S(1)}, bf16[2048,256]{1,0:T(8,128)(2,1)}, u32[]{:S(2)}) copy-start(bf16[2048,256]{1,0:T(8,128)(2,1)} %param.27) | copy-start | bytes 3145732
  6.5 257.8 %all-gather.5.cloned.1.call-start = ((), (), s32[]{:S(2)}) async-start(), calls=%async_computation.2 | async-start | bytes 5242880 | tf_op jit(solution)/shard_map/all_gather | solution.py:212
  84.2 2.8 %copy-start.5 = (f32[2]{0:T(128)S(1)}, f32[2]{0:T(128)}, u32[]{:S(2)}) copy-start(f32[2]{0:T(128)} %param.30) | copy-start | bytes 28
  84.3 2.9 %copy-start.8 = (f32[128]{0:T(128)S(1)}, f32[128]{0:T(128)}, u32[]{:S(2)}) copy-start(f32[128]{0:T(128)} %param.31) | copy-start | bytes 1540
  84.8 7.3 %copy-start.2 = (bf16[2048,256]{1,0:T(8,128)(2,1)S(1)}, bf16[2048,256]{1,0:T(8,128)(2,1)}, u32[]{:S(2)}) copy-start(bf16[2048,256]{1,0:T(8,128)(2,1)} %param.32) | copy-start | bytes 3145732
  85.4 8.9 %copy-start.6 = (f32[2,128,2]{1,2,0:T(2,128)S(1)}, f32[2,128,2]{1,2,0:T(2,128)}, u32[]{:S(2)}) copy-start(f32[2,128,2]{1,2,0:T(2,128)} %param.37) | copy-start | bytes 6148
  85.4 9.1 %copy-start.7 = (f32[2,256]{1,0:T(2,128)S(1)}, f32[2,256]{1,0:T(2,128)}, u32[]{:S(2)}) copy-start(f32[2,256]{1,0:T(2,128)} %param.36) | copy-start | bytes 6148
  88.1 168.7 %all-to-all-start = ((bf16[4,32,256]{2,1,0:T(8,128)(2,1)}), bf16[4,32,256]{2,1,0:T(8,128)(2,1)S(1)}, u32[]{:S(2)}, u32[]{:S(2)}) async-start(bf16[4,32,256]{2,1,0:T(8,128)(2,1)} %convert_element_type.144), calls=%async_computation | async-start | bytes 131072 | tf_op jit(solution)/shard_map/all_to_all | solution.py:207
  91.4 176.0 %all-gather.7.cloned.1.call-start = ((), (), s32[]{:S(2)}) async-start(), calls=%async_computation.3 | async-start | bytes 5242880 | tf_op jit(solution)/shard_map/all_gather | solution.py:216
  125.9 81.0 %copy-start.3 = (f32[2,2,128,128]{3,2,1,0:T(8,128)S(1)}, f32[2,2,128,128]{3,2,1,0:T(8,128)}, u32[]{:S(2)}) copy-start(f32[2,2,128,128]{3,2,1,0:T(8,128)} %param.38) | copy-start | bytes 786436
  153.5 102.4 %copy-start.9 = (f32[128]{0:T(128)S(1)}, f32[128]{0:T(128)}, u32[]{:S(2)}) copy-start(f32[128]{0:T(128)} %param.39) | copy-start | bytes 1540
  256.8 7.5 %all-to-all-start.1 = ((bf16[4,32,256]{2,1,0:T(8,128)(2,1)}), bf16[4,32,256]{2,1,0:T(8,128)(2,1)S(1)}, u32[]{:S(2)}, u32[]{:S(2)}) async-start(bf16[4,32,256]{2,1,0:T(8,128)(2,1)} %convert_element_type.160), calls=%async_computation.1 | async-start | bytes 131072 | tf_op jit(solution)/shard_map/all_to_all | solution.py:208
Sparse Core Ops, SparseCore 0:
  8.9 37.1 all-gather.4
  93.8 36.0 all-gather.6
where the time goes:
time: 278 us
  blocking collectives  171 us (62%)
  matrix products  47 us (17%)
  other arithmetic  27.7 us (10%)
  between operations  13.9 us (5%)
  starting transfers between devices  6.87 us (2%)
  waiting for transfers between devices  5.34 us (2%)
  local copies, waits for them, and re-layouts  4.9 us (2%)
    all_gather x4, blocking collectives, prefix(): lax.all_gather(a.astype(kind), axis)  99.4 us
    all_gather x1, blocking collectives, local(): value_piece = lax.all_gather(value_att, 'sp', axis=0, tiled=True)  31.9 us
    all_gather x1, blocking collectives, local(): key_piece = lax.all_gather(key_att, 'sp', axis=0, tiled=True)  31.2 us
    dot_general x4, matrix products, block_one_step(): jnp.einsum('ihk,ijhk,jhk->hij', query_tile, jnp.exp(relative), key_tile,...  26.5 us
    dot_general x4, other arithmetic, block_one_step(): jnp.einsum('ihk,ijhk,jhk->hij', query_tile, jnp.exp(relative), key_tile,...  23.6 us
    all_gather x1, blocking collectives, local(): lax.all_gather(tokens, 'tp', axis=1, tiled=True).astype(jnp.float32)  8.89 us
    dot_general x7, matrix products, local(): jnp.dot(scaled, weight, preferred_element_type=jnp.float32)  7.32 us
  transfers between devices with their start and end apart: 4, of which 1 were waited for; matrix products, arithmetic and copies ran while one was open for 27% of the time, Pallas kernels for 0%

commit v1 on v0

v1 whole, which is shorter than its diff:
```python
import functools

import jax
import jax.numpy as jnp
from jax import lax
from jax.experimental import pallas as pl
from jax.experimental.pallas import tpu as pltpu
from jax.sharding import PartitionSpec as P

QK_DIM = 64
DA_VAL = 128
HG = 128
BLOCK = 128
KEY_CHUNK = 1024
TAIL = 16
EPSILON = 1e-06
F32 = jnp.float32
BF16 = jnp.bfloat16
NT = (((1,), (1,)), ((), ()))
TN = (((0,), (0,)), ((), ()))


def dot(a, b, dims=(((1,), (0,)), ((), ())), precision=None):
    return lax.dot_general(a, b, dims, precision=precision, preferred_element_type=F32)


def kernel(
    line, tp_count, feats,
    tokens, gain, lam, attn_gain, gap, extra, init, rec_gain,
    w0, w1, w2, w3, w4, w5, w6, wa, wr,
    out,
    tok, sums, wbuf, wobuf, acc, kv, pq, rec_local, qdec, mine, other, pair_f, pair_b,
    partial, parts,
    w_sem, t_send, t_recv, up_send, up_recv, dn_send, dn_recv, x_send, x_recv,
    s_send, s_recv, su_send, su_recv, sd_send, sd_recv, o_send, o_recv,
):
    rows, fb = tokens.shape
    width = w0.shape[1]
    heads = width // HG
    sp = lax.axis_index("sp")
    tp = lax.axis_index("tp")
    z = sp // 2
    x = sp % 2
    sp_x = z * 2 + (1 - x)
    tp1 = tp + 1 - 2 * (tp % 2)
    tp2 = (tp + 2) % 4
    tp3 = 3 - tp
    has_up = z + 1 < line
    has_dn = z >= 1

    def dev(s, t):
        return (s, t)

    def remote(src, dst, ss, rs, to):
        return pltpu.make_async_remote_copy(
            src_ref=src, dst_ref=dst, send_sem=ss, recv_sem=rs,
            device_id=to, device_id_type=pl.DeviceIdType.MESH,
        )

    order = (1, 2, 0, 3, 4, 5, 6)
    weights = (w0, w1, w2, w3, w4, w5, w6)
    loads = {}
    for w in order:
        loads[w] = pltpu.make_async_copy(weights[w], wbuf.at[w], w_sem.at[w])
        loads[w].start()
    load_a = pltpu.make_async_copy(wa, wobuf.at[0], w_sem.at[7])
    load_r = pltpu.make_async_copy(wr, wobuf.at[1], w_sem.at[8])
    load_a.start()
    load_r.start()

    barrier = pltpu.get_barrier_semaphore()
    for t in (tp1, tp2, tp3):
        pl.semaphore_signal(barrier, inc=1, device_id=dev(sp, t), device_id_type=pl.DeviceIdType.MESH)
    pl.semaphore_signal(barrier, inc=1, device_id=dev(sp_x, tp), device_id_type=pl.DeviceIdType.MESH)

    @pl.when(has_up)
    def _():
        pl.semaphore_signal(barrier, inc=1, device_id=dev(sp + 2, tp), device_id_type=pl.DeviceIdType.MESH)

    @pl.when(has_dn)
    def _():
        pl.semaphore_signal(barrier, inc=1, device_id=dev(sp - 2, tp), device_id_type=pl.DeviceIdType.MESH)

    pl.semaphore_wait(barrier, 4 + has_up.astype(jnp.int32) + has_dn.astype(jnp.int32))

    to_y = remote(tokens, tok.at[tp], t_send.at[0], t_recv.at[0], dev(sp, tp2))
    to_1 = remote(tokens, tok.at[tp], t_send.at[1], t_recv.at[1], dev(sp, tp1))
    on_1 = remote(tok.at[tp2], tok.at[tp2], t_send.at[2], t_recv.at[2], dev(sp, tp1))
    to_y.start()
    to_1.start()

    def scaled_of(ref, owner):
        v = ref[...].astype(F32)
        sq = jnp.sum(v * v, axis=1, keepdims=True)
        g = gain[0:1, pl.ds(pl.multiple_of(owner * fb, fb), fb)]
        return (v * g).astype(BF16), sq

    def product(s, owner, w):
        return dot(s, wbuf[w, pl.ds(pl.multiple_of(owner * fb, fb), fb), :])

    def col(w):
        return slice(w * width, (w + 1) * width)

    s, sq0 = scaled_of(tokens, tp)
    for w in order:
        loads[w].wait()
        acc[:, col(w)] = product(s, tp, w)
    to_1.wait_recv()
    s, sq1 = scaled_of(tok.at[tp1], tp1)
    for w in order:
        acc[:, col(w)] += product(s, tp1, w)
    to_y.wait_recv()
    on_1.start()
    s, sq2 = scaled_of(tok.at[tp2], tp2)
    for w in order:
        acc[:, col(w)] += product(s, tp2, w)
    on_1.wait_recv()
    s, sq3 = scaled_of(tok.at[tp3], tp3)
    inv = lax.rsqrt((sq0 + sq1 + sq2 + sq3) / feats + EPSILON)

    def project(w):
        return ((acc[:, col(w)] + product(s, tp3, w)) * inv).astype(BF16)

    kv[sp, :, :width] = project(1)
    kv[sp, :, width:] = project(2)

    def up(h):
        slot = sp - 2 * (h - 1)
        return remote(kv.at[slot], kv.at[slot], up_send.at[h], up_recv.at[h], dev(sp + 2, tp))

    def dn(h):
        slot = sp + 2 * (h - 1)
        return remote(kv.at[slot], kv.at[slot], dn_send.at[h], dn_recv.at[h], dev(sp - 2, tp))

    def across(slot, k):
        return remote(kv.at[slot], kv.at[slot], x_send.at[k], x_recv.at[k], dev(sp_x, tp))

    pl.when(has_up)(lambda: up(1).start())
    pl.when(has_dn)(lambda: dn(1).start())
    across(sp, 0).start()

    pq[...] = (project(0).astype(F32) * QK_DIM ** -0.5).astype(BF16)
    rq = project(3).astype(F32)
    forgets = (project(4).astype(F32), project(5).astype(F32))
    rv = project(6)
    q_all = rq / (1.0 + jnp.exp(-rq)) * HG ** -0.5

    blocks = rows // BLOCK
    r_id = lax.broadcasted_iota(jnp.int32, (BLOCK, BLOCK), 0)
    c_id = lax.broadcasted_iota(jnp.int32, (BLOCK, BLOCK), 1)
    for d in range(2):
        mask = c_id <= r_id if d == 0 else c_id >= r_id
        tri = mask.astype(F32)
        key_all = gap[d : d + 1, :] / (1.0 + jnp.exp(forgets[d]))
        lg_all = jnp.log1p(-key_all)
        states = [None] * heads
        totals = [None] * heads
        for b in range(blocks) if d == 0 else reversed(range(blocks)):
            rs = slice(b * BLOCK, (b + 1) * BLOCK)
            for h in range(heads):
                hs = slice(h * HG, (h + 1) * HG)
                g = lg_all[rs, hs] + extra[d, rs, h : h + 1]
                c = dot(tri, g, precision=lax.Precision.HIGHEST)
                end = c[BLOCK - 1 : BLOCK] if d == 0 else c[0:1]
                mid = end * 0.5
                q = q_all[rs, hs]
                k = key_all[rs, hs]
                v = rv[rs, hs]
                scores = dot((q * jnp.exp(c - mid)).astype(BF16), (k * jnp.exp(mid - c)).astype(BF16), NT)
                scores = jnp.where(mask, scores, 0.0).astype(BF16)
                res = dot(scores, v)
                add = dot(v, (k * jnp.exp(end - c)).astype(BF16), TN)
                if states[h] is None:
                    qdec[d, rs, hs] = (q * jnp.exp(c)).astype(BF16)
                    states[h] = add
                    totals[h] = end
                else:
                    res = res + dot((q * jnp.exp(c)).astype(BF16), states[h].astype(BF16), NT)
                    qdec[d, rs, hs] = (q * jnp.exp(c + totals[h])).astype(BF16)
                    states[h] = states[h] * jnp.exp(end) + add
                    totals[h] = totals[h] + end
                if d == 0:
                    rec_local[rs, hs] = res
                else:
                    rec_local[rs, hs] += res
        store_state(mine.at[d], states, totals, heads)

    swap = remote(mine, other, s_send.at[0], s_recv.at[0], dev(sp_x, tp))
    swap.start()

    def receive(h):
        @pl.when(z >= h)
        def _():
            up(h).wait_recv()
            pl.when(has_up)(lambda: up(h + 1).start())
            across(sp - 2 * h, h).start()

        @pl.when(z + h < line)
        def _():
            dn(h).wait_recv()
            pl.when(has_dn)(lambda: dn(h + 1).start())
            across(sp + 2 * h, line - 1 + h).start()

    if line > 1:
        receive(1)

    swap.wait_recv()
    for d in range(2):
        s_mine, l_mine = load_state(mine.at[d], heads)
        s_other, l_other = load_state(other.at[d], heads)
        first_is_mine = x == d
        pairs, logs = [], []
        for h in range(heads):
            early = jnp.where(first_is_mine, s_mine[h], s_other[h])
            late = jnp.where(first_is_mine, s_other[h], s_mine[h])
            l_late = jnp.where(first_is_mine, l_other[h], l_mine[h])
            pairs.append(early * jnp.exp(l_late) + late)
            logs.append(l_mine[h] + l_other[h])
        store_state((pair_f if d == 0 else pair_b).at[z], pairs, logs, heads)

    def s_up(h):
        slot = z - (h - 1)
        return remote(pair_f.at[slot], pair_f.at[slot], su_send.at[h], su_recv.at[h], dev(sp + 2, tp))

    def s_dn(h):
        slot = z + (h - 1)
        return remote(pair_b.at[slot], pair_b.at[slot], sd_send.at[h], sd_recv.at[h], dev(sp - 2, tp))

    pl.when(has_up)(lambda: s_up(1).start())
    pl.when(has_dn)(lambda: s_dn(1).start())

    for h in range(1, line):
        if h > 1:
            receive(h)

        @pl.when(z >= h)
        def _(h=h):
            s_up(h).wait_recv()
            pl.when(has_up)(lambda: s_up(h + 1).start())

        @pl.when(z + h < line)
        def _(h=h):
            s_dn(h).wait_recv()
            pl.when(has_dn)(lambda: s_dn(h + 1).start())

    for d in range(2):
        buf = pair_f if d == 0 else pair_b

        def fold(i, carry, d=d, buf=buf):
            st, lg = load_state(buf.at[i if d == 0 else line - 1 - i], heads)
            return tuple(carry[h] * jnp.exp(lg[h]) + st[h] for h in range(heads))

        start = tuple(init[d, h].T for h in range(heads))
        enter = lax.fori_loop(0, z if d == 0 else line - 1 - z, fold, start)
        st, lg = load_state(other.at[d], heads)
        for h in range(heads):
            hs = slice(h * HG, (h + 1) * HG)
            e = jnp.where(x == 1 - d, enter[h] * jnp.exp(lg[h]) + st[h], enter[h])
            rec_local[:, hs] += dot(qdec[d, :, hs], e.astype(BF16), NT)
    rec_out = []
    for h in range(heads):
        r = rec_local[:, h * HG : (h + 1) * HG]
        n = r * lax.rsqrt(jnp.mean(r * r, axis=1, keepdims=True) + EPSILON) * rec_gain[...]
        rec_out.append(n.astype(BF16))

    across(sp, 0).wait_recv()
    for h in range(1, line):
        pl.when(z >= h)(lambda h=h: across(sp - 2 * h, h).wait_recv())
        pl.when(z + h < line)(lambda h=h: across(sp + 2 * h, line - 1 + h).wait_recv())

    slots = 2 * line
    per = max(c for c in range(1, slots + 1) if slots % c == 0 and c * rows <= max(KEY_CHUNK, rows))
    attn_out = []
    lane = lax.broadcasted_iota(jnp.int32, (rows, DA_VAL), 1)
    for h in range(heads):
        hs = slice(h * DA_VAL, (h + 1) * DA_VAL)
        vs = slice(width + h * DA_VAL, width + (h + 1) * DA_VAL)
        q = pq[:, hs].astype(F32)
        q = jnp.concatenate(
            [jnp.where(lane < QK_DIM, q, 0.0), jnp.where(lane >= QK_DIM, q, 0.0)], axis=0
        ).astype(BF16)

        def part(i, q=q, hs=hs, vs=vs):
            block = pl.ds(i * per, per)
            k = kv[block, :, hs].reshape(per * rows, DA_VAL)
            v = kv[block, :, vs].reshape(per * rows, DA_VAL)
            sc = dot(q, k, NT)
            m = jnp.max(sc, axis=1, keepdims=True)
            e = jnp.exp(sc - m)
            return m, jnp.sum(e, axis=1, keepdims=True), dot(e.astype(BF16), v)

        def absorb(i, carry, part=part):
            m0, d0, n0 = carry
            m1, d1, n1 = part(i)
            m = jnp.maximum(m0, m1)
            f0, f1 = jnp.exp(m0 - m), jnp.exp(m1 - m)
            return m, d0 * f0 + d1 * f1, n0 * f0 + n1 * f1

        carry = part(0)
        if slots // per > 1:
            carry = lax.fori_loop(1, slots // per, absorb, carry)
        ratio = carry[2] / carry[1]
        diff = ratio[:rows] - lam[0, h] * ratio[rows:]
        n = diff * lax.rsqrt(jnp.mean(diff * diff, axis=1, keepdims=True) + EPSILON) * attn_gain[...]
        attn_out.append(n.astype(BF16))

    load_a.wait()
    load_r.wait()
    a_all = jnp.concatenate(attn_out, axis=1)
    r_all = jnp.concatenate(rec_out, axis=1)
    own = rows // tp_count
    chunks = partial.shape[0]
    cw = partial.shape[2]
    peers = (tp3, tp2, tp1)

    def send(j, i):
        return remote(
            partial.at[j, pl.ds(pl.multiple_of(peers[i] * own, own), own)], parts.at[j, i],
            o_send.at[3 * j + i], o_recv.at[3 * j + i], dev(sp, peers[i]),
        )

    for j in range(chunks):
        cs = slice(j * cw, (j + 1) * cw)
        partial[j] = (dot(a_all, wobuf[0, :, cs]) + dot(r_all, wobuf[1, :, cs])).astype(BF16)
        for i in range(3):
            send(j, i).start()
    mine_rows = pl.ds(pl.multiple_of(tp * own, own), own)
    for j in range(chunks):
        total = partial[j, mine_rows, :].astype(F32)
        for i in range(3):
            send(j, i).wait_recv()
            total = total + parts[j, i].astype(F32)
        out[:, j * cw : (j + 1) * cw] = total.astype(BF16)

    to_y.wait_send()
    to_1.wait_send()
    on_1.wait_send()
    swap.wait_send()
    across(sp, 0).wait_send()
    for h in range(1, line):
        @pl.when(jnp.logical_and(has_up, z >= h - 1))
        def _(h=h):
            up(h).wait_send()
            s_up(h).wait_send()

        @pl.when(jnp.logical_and(has_dn, z + h - 1 < line))
        def _(h=h):
            dn(h).wait_send()
            s_dn(h).wait_send()

        pl.when(z >= h)(lambda h=h: across(sp - 2 * h, h).wait_send())
        pl.when(z + h < line)(lambda h=h: across(sp + 2 * h, line - 1 + h).wait_send())
    for j in range(chunks):
        for i in range(3):
            send(j, i).wait_send()


def store_state(ref, states, logs, heads):
    for h in range(heads):
        ref[h * HG : (h + 1) * HG, :] = states[h].astype(BF16)
    high = [l.astype(BF16).astype(F32) for l in logs]
    low = [l - hi for l, hi in zip(logs, high)]
    row = lax.broadcasted_iota(jnp.int32, (TAIL, HG), 0)
    tail = jnp.zeros((TAIL, HG), F32)
    for i, value in enumerate(high + low):
        tail = jnp.where(row == i, value, tail)
    ref[heads * HG : heads * HG + TAIL, :] = tail.astype(BF16)


def load_state(ref, heads):
    states = [ref[h * HG : (h + 1) * HG, :].astype(F32) for h in range(heads)]
    tail = ref[heads * HG : heads * HG + TAIL, :].astype(F32)
    logs = [tail[h : h + 1] + tail[heads + h : heads + h + 1] for h in range(heads)]
    return states, logs


def solution(mesh):
    sp_count = mesh.shape["sp"]
    tp_count = mesh.shape["tp"]
    line = sp_count // 2

    def local(
        tokens, norm_gain, da_query, da_key, da_value, mix_lambda, attn_gain,
        rec_query, rec_forget_fwd, rec_forget_bwd, rec_value,
        gate_gap, extra_decay, init_state, rec_gain, out_attn, out_rec,
    ):
        rows, fb = tokens.shape
        feats, width = da_query.shape
        heads = width // HG
        columns = out_attn.shape[1]
        own = rows // tp_count
        chunks = 4
        cw = columns // chunks
        state = (heads * HG + TAIL, HG)
        vm = pl.BlockSpec(memory_space=pltpu.VMEM)
        sm = pl.BlockSpec(memory_space=pltpu.SMEM)
        hb = pl.BlockSpec(memory_space=pl.ANY)
        dma = pltpu.SemaphoreType.DMA
        return pl.pallas_call(
            functools.partial(kernel, line, tp_count, feats),
            out_shape=jax.ShapeDtypeStruct((own, columns), BF16),
            in_specs=[vm, vm, sm, vm, vm, vm, vm, vm] + [hb] * 9,
            out_specs=vm,
            scratch_shapes=[
                pltpu.VMEM((tp_count, rows, fb), BF16),
                pltpu.VMEM((8, 128), F32),
                pltpu.VMEM((7, feats, width), BF16),
                pltpu.VMEM((2, width, columns), BF16),
                pltpu.VMEM((rows, 7 * width), F32),
                pltpu.VMEM((sp_count, rows, 2 * width), BF16),
                pltpu.VMEM((rows, width), BF16),
                pltpu.VMEM((rows, width), F32),
                pltpu.VMEM((2, rows, width), BF16),
                pltpu.VMEM((2,) + state, BF16),
                pltpu.VMEM((2,) + state, BF16),
                pltpu.VMEM((line,) + state, BF16),
                pltpu.VMEM((line,) + state, BF16),
                pltpu.VMEM((chunks, rows, cw), BF16),
                pltpu.VMEM((chunks, 3, own, cw), BF16),
                dma((9,)), dma((3,)), dma((3,)),
                dma((line + 1,)), dma((line + 1,)), dma((line + 1,)), dma((line + 1,)),
                dma((2 * line,)), dma((2 * line,)),
                dma((1,)), dma((1,)),
                dma((line + 1,)), dma((line + 1,)), dma((line + 1,)), dma((line + 1,)),
                dma((3 * chunks,)), dma((3 * chunks,)),
            ],
            compiler_params=pltpu.CompilerParams(
                collective_id=0, has_side_effects=True, vmem_limit_bytes=60 * 1024 * 1024
            ),
        )(
            tokens, norm_gain.reshape(1, -1), mix_lambda.reshape(1, -1), attn_gain.reshape(1, -1),
            gate_gap, extra_decay, init_state, rec_gain.reshape(1, -1),
            da_query, da_key, da_value, rec_query, rec_forget_fwd, rec_forget_bwd, rec_value,
            out_attn, out_rec,
        )

    placed = (
        P("sp", "tp"), P(), P(None, "tp"), P(None, "tp"), P(None, "tp"), P("tp"), P(),
        P(None, "tp"), P(None, "tp"), P(None, "tp"), P(None, "tp"), P(None, "tp"),
        P(None, "sp", "tp"), P(None, "tp", None, None), P(), P("tp", None), P("tp", None),
    )
    return jax.shard_map(
        local, mesh=mesh, in_specs=placed, out_specs=P(("sp", "tp"), None), check_vma=False
    )
```

time: 278 us -> 45.7 us (0.16)
  blocking collectives: 171 us -> 0 us
  matrix products: 47 us -> 0 us
  Pallas kernels: 0 us -> 42.5 us
  other arithmetic: 27.7 us -> 0 us
  between operations: 13.9 us -> 0.01 us
  starting transfers between devices: 6.87 us -> 0 us
  waiting for transfers between devices: 5.34 us -> 0 us
    all_gather x7 -> x0, blocking collectives: 171 us -> none  [the longest x4 99.4 us: prefix(): lax.all_gather(a.astype(kind), axis)]
    dot_general x29 -> x0, matrix products: 47 us -> none  [the longest x4 26.5 us: block_one_step(): jnp.einsum('ihk,ijhk,jhk->hij', query_tile, jnp.exp(relative), key_tile,...]
    pallas_call x0 -> x1, Pallas kernels: none -> 42.5 us  [local(): pl.pallas_call(functools.partial(kernel, line, tp_count, feats), out_shap...]
    dot_general x4 -> x0, other arithmetic: 23.6 us -> none  [block_one_step(): jnp.einsum('ihk,ijhk,jhk->hij', query_tile, jnp.exp(relative), key_tile,...]
    all_to_all x2 -> x0, starting transfers between devices: 6.65 us -> none  [the longest x1 3.37 us: local(): lax.all_to_all(rec_out, 'tp', split_axis=0, concat_axis=1, tiled=True)]
    all_to_all x2 -> x0, waiting for transfers between devices: 4.12 us -> none  [the longest x1 4.11 us: local(): lax.all_to_all(rec_out, 'tp', split_axis=0, concat_axis=1, tiled=True)]
    unnamed x20 -> x4, local copies, waits for them, and re-layouts: 0.05 us -> 3.05 us
  transfers between devices with their start and end apart: 4 -> 0, of which waited for: 1 -> 0; matrix products, arithmetic and copies ran while one was open for 27% -> 0% of each run, Pallas kernels for 0% -> 0%
where the time goes in v1:
time: 45.7 us; the launch traced here: 45.5 us
  Pallas kernels  42.5 us (93%)
  local copies, waits for them, and re-layouts  3.05 us (7%)
    pallas_call x1, Pallas kernels, local(): pl.pallas_call(functools.partial(kernel, line, tp_count, feats), out_shap...  42.5 us
    unnamed x4, local copies, waits for them, and re-layouts  3.05 us

profile of v1, /device:TPU:0, one launch (start us, length us, event | category | flops | bytes accessed | tf_op | source)
XLA Modules:
  0.0 45.5 jit_solution(8104109305210019536)
XLA Ops:
  0.0 0.0 copy-start
  0.0 0.7 %copy-done = f32[2,128,2]{1,2,0:T(2,128)S(1)} copy-done((f32[2,128,2]{1,2,0:T(2,128)S(1)}, f32[2,128,2]{1,2,0:T(2,128)}, u32[]{:S(2)}) %copy-start) | copy-done | bytes 2072
  0.7 0.8 %copy.18.extra = f32[2,128,2]{2,1,0:T(8,128)} copy(f32[2,128,2]{1,2,0:T(2,128)S(1)} %copy-done) | data formatting | bytes 4096 | tf_op args[12]
  1.5 42.5 %shard_map.163 = bf16[32,2048]{1,0:T(8,128)(2,1)} custom-call(bf16[128,512]{1,0:T(8,128)(2,1)} %tokens.1, f32[1,2048]{1,0:T(1,128)} %bitcast.4, f32[1,2]{1,0:T(1,128)} %bitcast.5, f32[1,128]{1,0:T(1,128)} %bitcast.6, f32[2,256]{1,0:T(2,128)} %gap.1, f32[2,128,2]{2,1,0:T(8,128)} %copy.18.extra, f32[2,2,128,128]{3,2,1,0:T(8,128)} %init.1, f32[1,128]{1,0:T(1,128)} %bitcast.7, ...), custom_call_target="tpu_custom_call" | custom-call | tf_op jit(solution)/shard_map/pallas_call | solution.py:399
  44.0 1.6 %copy.20 = bf16[32,2048]{1,0:T(8,128)(2,1)} copy(bf16[32,2048]{1,0:T(8,128)(2,1)} %shard_map.163) | data formatting | bytes 262144
Async XLA Ops:
  0.0 0.7 %copy-start = (f32[2,128,2]{1,2,0:T(2,128)S(1)}, f32[2,128,2]{1,2,0:T(2,128)}, u32[]{:S(2)}) copy-start(f32[2,128,2]{1,2,0:T(2,128)} %param.29) | copy-start | bytes 6148

commit v2 on v1

--- a/solution.py
+++ b/solution.py
@@ -26,12 +26,12 @@
 
 def kernel(
     line, tp_count, feats,
-    tokens, gain, lam, attn_gain, gap, extra, init, rec_gain,
+    tokens, gain_h, lam, attn_gain_h, gap_h, extra_h, init_h, rec_gain_h,
     w0, w1, w2, w3, w4, w5, w6, wa, wr,
     out,
-    tok, sums, wbuf, wobuf, acc, kv, pq, rec_local, qdec, mine, other, pair_f, pair_b,
+    gain, attn_gain, gap, extra, init, rec_gain, tok, wbuf, wobuf, acc, kv, pq, rec_local, qdec, mine, other, pair_f, pair_b,
     partial, parts,
-    w_sem, t_send, t_recv, up_send, up_recv, dn_send, dn_recv, x_send, x_recv,
+    in_sem, w_sem, t_send, t_recv, up_send, up_recv, dn_send, dn_recv, x_send, x_recv,
     s_send, s_recv, su_send, su_recv, sd_send, sd_recv, o_send, o_recv,
 ):
     rows, fb = tokens.shape
@@ -57,6 +57,13 @@
             device_id=to, device_id_type=pl.DeviceIdType.MESH,
         )
 
+    load_t = pltpu.make_async_copy(tokens, tok.at[tp], in_sem.at[0])
+    load_t.start()
+    smalls = []
+    pairs_in = ((gain_h, gain), (extra_h, extra), (gap_h, gap), (init_h, init), (attn_gain_h, attn_gain), (rec_gain_h, rec_gain))
+    for i, (a, b) in enumerate(pairs_in):
+        smalls.append(pltpu.make_async_copy(a, b, in_sem.at[i + 1]))
+    smalls[0].start()
     order = (1, 2, 0, 3, 4, 5, 6)
     weights = (w0, w1, w2, w3, w4, w5, w6)
     loads = {}
@@ -67,24 +74,23 @@
     load_r = pltpu.make_async_copy(wr, wobuf.at[1], w_sem.at[8])
     load_a.start()
     load_r.start()
+    for c in smalls[1:]:
+        c.start()
 
     barrier = pltpu.get_barrier_semaphore()
     for t in (tp1, tp2, tp3):
         pl.semaphore_signal(barrier, inc=1, device_id=dev(sp, t), device_id_type=pl.DeviceIdType.MESH)
     pl.semaphore_signal(barrier, inc=1, device_id=dev(sp_x, tp), device_id_type=pl.DeviceIdType.MESH)
-
-    @pl.when(has_up)
-    def _():
-        pl.semaphore_signal(barrier, inc=1, device_id=dev(sp + 2, tp), device_id_type=pl.DeviceIdType.MESH)
-
-    @pl.when(has_dn)
-    def _():
-        pl.semaphore_signal(barrier, inc=1, device_id=dev(sp - 2, tp), device_id_type=pl.DeviceIdType.MESH)
-
-    pl.semaphore_wait(barrier, 4 + has_up.astype(jnp.int32) + has_dn.astype(jnp.int32))
-
-    to_y = remote(tokens, tok.at[tp], t_send.at[0], t_recv.at[0], dev(sp, tp2))
-    to_1 = remote(tokens, tok.at[tp], t_send.at[1], t_recv.at[1], dev(sp, tp1))
+    for h in range(1, line):
+        other_z = lax.rem(z + h, line)
+        pl.semaphore_signal(
+            barrier, inc=1, device_id=dev(other_z * 2 + x, tp), device_id_type=pl.DeviceIdType.MESH
+        )
+    load_t.wait()
+    pl.semaphore_wait(barrier, 4 + line - 1)
+
+    to_y = remote(tok.at[tp], tok.at[tp], t_send.at[0], t_recv.at[0], dev(sp, tp2))
+    to_1 = remote(tok.at[tp], tok.at[tp], t_send.at[1], t_recv.at[1], dev(sp, tp1))
     on_1 = remote(tok.at[tp2], tok.at[tp2], t_send.at[2], t_recv.at[2], dev(sp, tp1))
     to_y.start()
     to_1.start()
@@ -101,7 +107,8 @@
     def col(w):
         return slice(w * width, (w + 1) * width)
 
-    s, sq0 = scaled_of(tokens, tp)
+    smalls[0].wait()
+    s, sq0 = scaled_of(tok.at[tp], tp)
     for w in order:
         loads[w].wait()
         acc[:, col(w)] = product(s, tp, w)
@@ -121,23 +128,26 @@
     def project(w):
         return ((acc[:, col(w)] + product(s, tp3, w)) * inv).astype(BF16)
 
-    kv[sp, :, :width] = project(1)
-    kv[sp, :, width:] = project(2)
-
-    def up(h):
+    def up(p, h):
         slot = sp - 2 * (h - 1)
-        return remote(kv.at[slot], kv.at[slot], up_send.at[h], up_recv.at[h], dev(sp + 2, tp))
-
-    def dn(h):
+        i = p * (line + 1) + h
+        return remote(kv.at[p, slot], kv.at[p, slot], up_send.at[i], up_recv.at[i], dev(sp + 2, tp))
+
+    def dn(p, h):
         slot = sp + 2 * (h - 1)
-        return remote(kv.at[slot], kv.at[slot], dn_send.at[h], dn_recv.at[h], dev(sp - 2, tp))
-
-    def across(slot, k):
-        return remote(kv.at[slot], kv.at[slot], x_send.at[k], x_recv.at[k], dev(sp_x, tp))
-
-    pl.when(has_up)(lambda: up(1).start())
-    pl.when(has_dn)(lambda: dn(1).start())
-    across(sp, 0).start()
+        i = p * (line + 1) + h
+        return remote(kv.at[p, slot], kv.at[p, slot], dn_send.at[i], dn_recv.at[i], dev(sp - 2, tp))
+
+    def across(p, slot, k):
+        i = p * 2 * line + k
+        return remote(kv.at[p, slot], kv.at[p, slot], x_send.at[i], x_recv.at[i], dev(sp_x, tp))
+
+    for p in range(2):
+        kv[p, sp] = project(1 + p)
+        pl.when(has_up)(lambda: up(p, 1).start())
+        pl.when(has_dn)(lambda: dn(p, 1).start())
+        if p == 0:
+            across(0, sp, 0).start()
 
     pq[...] = (project(0).astype(F32) * QK_DIM ** -0.5).astype(BF16)
     rq = project(3).astype(F32)
@@ -145,6 +155,8 @@
     rv = project(6)
     q_all = rq / (1.0 + jnp.exp(-rq)) * HG ** -0.5
 
+    for c in smalls[1:]:
+        c.wait()
     blocks = rows // BLOCK
     r_id = lax.broadcasted_iota(jnp.int32, (BLOCK, BLOCK), 0)
     c_id = lax.broadcasted_iota(jnp.int32, (BLOCK, BLOCK), 1)
@@ -159,7 +171,7 @@
             rs = slice(b * BLOCK, (b + 1) * BLOCK)
             for h in range(heads):
                 hs = slice(h * HG, (h + 1) * HG)
-                g = lg_all[rs, hs] + extra[d, rs, h : h + 1]
+                g = lg_all[rs, hs] + jnp.broadcast_to(extra[d, h : h + 1, rs], (HG, BLOCK)).T
                 c = dot(tri, g, precision=lax.Precision.HIGHEST)
                 end = c[BLOCK - 1 : BLOCK] if d == 0 else c[0:1]
                 mid = end * 0.5
@@ -187,19 +199,21 @@
 
     swap = remote(mine, other, s_send.at[0], s_recv.at[0], dev(sp_x, tp))
     swap.start()
+    across(1, sp, 0).start()
 
     def receive(h):
-        @pl.when(z >= h)
-        def _():
-            up(h).wait_recv()
-            pl.when(has_up)(lambda: up(h + 1).start())
-            across(sp - 2 * h, h).start()
-
-        @pl.when(z + h < line)
-        def _():
-            dn(h).wait_recv()
-            pl.when(has_dn)(lambda: dn(h + 1).start())
-            across(sp + 2 * h, line - 1 + h).start()
+        for p in range(2):
+            @pl.when(z >= h)
+            def _(p=p):
+                up(p, h).wait_recv()
+                pl.when(has_up)(lambda: up(p, h + 1).start())
+                across(p, sp - 2 * h, h).start()
+
+            @pl.when(z + h < line)
+            def _(p=p):
+                dn(p, h).wait_recv()
+                pl.when(has_dn)(lambda: dn(p, h + 1).start())
+                across(p, sp + 2 * h, line - 1 + h).start()
 
     if line > 1:
         receive(1)
@@ -218,30 +232,20 @@
             logs.append(l_mine[h] + l_other[h])
         store_state((pair_f if d == 0 else pair_b).at[z], pairs, logs, heads)
 
-    def s_up(h):
-        slot = z - (h - 1)
-        return remote(pair_f.at[slot], pair_f.at[slot], su_send.at[h], su_recv.at[h], dev(sp + 2, tp))
-
-    def s_dn(h):
-        slot = z + (h - 1)
-        return remote(pair_b.at[slot], pair_b.at[slot], sd_send.at[h], sd_recv.at[h], dev(sp - 2, tp))
-
-    pl.when(has_up)(lambda: s_up(1).start())
-    pl.when(has_dn)(lambda: s_dn(1).start())
+    def s_up(slot, h):
+        return remote(pair_f.at[slot], pair_f.at[slot], su_send.at[h], su_recv.at[h], dev(sp + 2 * h, tp))
+
+    def s_dn(slot, h):
+        return remote(pair_b.at[slot], pair_b.at[slot], sd_send.at[h], sd_recv.at[h], dev(sp - 2 * h, tp))
 
     for h in range(1, line):
-        if h > 1:
-            receive(h)
-
-        @pl.when(z >= h)
-        def _(h=h):
-            s_up(h).wait_recv()
-            pl.when(has_up)(lambda: s_up(h + 1).start())
-
-        @pl.when(z + h < line)
-        def _(h=h):
-            s_dn(h).wait_recv()
-            pl.when(has_dn)(lambda: s_dn(h + 1).start())
+        pl.when(z + h < line)(lambda h=h: s_up(z, h).start())
+        pl.when(z >= h)(lambda h=h: s_dn(z, h).start())
+    for h in range(2, line):
+        receive(h)
+    for h in range(1, line):
+        pl.when(z >= h)(lambda h=h: s_up(z - h, h).wait_recv())
+        pl.when(z + h < line)(lambda h=h: s_dn(z + h, h).wait_recv())
 
     for d in range(2):
         buf = pair_f if d == 0 else pair_b
@@ -263,10 +267,11 @@
         n = r * lax.rsqrt(jnp.mean(r * r, axis=1, keepdims=True) + EPSILON) * rec_gain[...]
         rec_out.append(n.astype(BF16))
 
-    across(sp, 0).wait_recv()
-    for h in range(1, line):
-        pl.when(z >= h)(lambda h=h: across(sp - 2 * h, h).wait_recv())
-        pl.when(z + h < line)(lambda h=h: across(sp + 2 * h, line - 1 + h).wait_recv())
+    for p in range(2):
+        across(p, sp, 0).wait_recv()
+        for h in range(1, line):
+            pl.when(z >= h)(lambda: across(p, sp - 2 * h, h).wait_recv())
+            pl.when(z + h < line)(lambda: across(p, sp + 2 * h, line - 1 + h).wait_recv())
 
     slots = 2 * line
     per = max(c for c in range(1, slots + 1) if slots % c == 0 and c * rows <= max(KEY_CHUNK, rows))
@@ -274,16 +279,15 @@
     lane = lax.broadcasted_iota(jnp.int32, (rows, DA_VAL), 1)
     for h in range(heads):
         hs = slice(h * DA_VAL, (h + 1) * DA_VAL)
-        vs = slice(width + h * DA_VAL, width + (h + 1) * DA_VAL)
         q = pq[:, hs].astype(F32)
         q = jnp.concatenate(
             [jnp.where(lane < QK_DIM, q, 0.0), jnp.where(lane >= QK_DIM, q, 0.0)], axis=0
         ).astype(BF16)
 
-        def part(i, q=q, hs=hs, vs=vs):
+        def part(i, q=q, hs=hs):
             block = pl.ds(i * per, per)
-            k = kv[block, :, hs].reshape(per * rows, DA_VAL)
-            v = kv[block, :, vs].reshape(per * rows, DA_VAL)
+            k = kv[0, block, :, hs].reshape(per * rows, DA_VAL)
+            v = kv[1, block, :, hs].reshape(per * rows, DA_VAL)
             sc = dot(q, k, NT)
             m = jnp.max(sc, axis=1, keepdims=True)
             e = jnp.exp(sc - m)
@@ -336,20 +340,16 @@
     to_1.wait_send()
     on_1.wait_send()
     swap.wait_send()
-    across(sp, 0).wait_send()
+    for p in range(2):
+        across(p, sp, 0).wait_send()
+        for h in range(1, line):
+            pl.when(jnp.logical_and(has_up, z >= h - 1))(lambda: up(p, h).wait_send())
+            pl.when(jnp.logical_and(has_dn, z + h - 1 < line))(lambda: dn(p, h).wait_send())
+            pl.when(z >= h)(lambda: across(p, sp - 2 * h, h).wait_send())
+            pl.when(z + h < line)(lambda: across(p, sp + 2 * h, line - 1 + h).wait_send())
     for h in range(1, line):
-        @pl.when(jnp.logical_and(has_up, z >= h - 1))
-        def _(h=h):
-            up(h).wait_send()
-            s_up(h).wait_send()
-
-        @pl.when(jnp.logical_and(has_dn, z + h - 1 < line))
-        def _(h=h):
-            dn(h).wait_send()
-            s_dn(h).wait_send()
-
-        pl.when(z >= h)(lambda h=h: across(sp - 2 * h, h).wait_send())
-        pl.when(z + h < line)(lambda h=h: across(sp + 2 * h, line - 1 + h).wait_send())
+        pl.when(z + h < line)(lambda h=h: s_up(z, h).wait_send())
+        pl.when(z >= h)(lambda h=h: s_dn(z, h).wait_send())
     for j in range(chunks):
         for i in range(3):
             send(j, i).wait_send()
@@ -394,20 +394,25 @@
         state = (heads * HG + TAIL, HG)
         vm = pl.BlockSpec(memory_space=pltpu.VMEM)
         sm = pl.BlockSpec(memory_space=pltpu.SMEM)
-        hb = pl.BlockSpec(memory_space=pl.ANY)
+        hb = pl.BlockSpec(memory_space=pltpu.HBM)
         dma = pltpu.SemaphoreType.DMA
         return pl.pallas_call(
             functools.partial(kernel, line, tp_count, feats),
             out_shape=jax.ShapeDtypeStruct((own, columns), BF16),
-            in_specs=[vm, vm, sm, vm, vm, vm, vm, vm] + [hb] * 9,
+            in_specs=[hb, hb, sm, hb, hb, hb, hb, hb] + [hb] * 9,
             out_specs=vm,
             scratch_shapes=[
+                pltpu.VMEM((1, norm_gain.shape[0]), F32),
+                pltpu.VMEM((1, attn_gain.shape[0]), F32),
+                pltpu.VMEM(gate_gap.shape, F32),
+                pltpu.VMEM((2, heads, rows), F32),
+                pltpu.VMEM(init_state.shape, F32),
+                pltpu.VMEM((1, rec_gain.shape[0]), F32),
                 pltpu.VMEM((tp_count, rows, fb), BF16),
-                pltpu.VMEM((8, 128), F32),
                 pltpu.VMEM((7, feats, width), BF16),
                 pltpu.VMEM((2, width, columns), BF16),
                 pltpu.VMEM((rows, 7 * width), F32),
-                pltpu.VMEM((sp_count, rows, 2 * width), BF16),
+                pltpu.VMEM((2, sp_count, rows, width), BF16),
                 pltpu.VMEM((rows, width), BF16),
                 pltpu.VMEM((rows, width), F32),
                 pltpu.VMEM((2, rows, width), BF16),
@@ -417,19 +422,19 @@
                 pltpu.VMEM((line,) + state, BF16),
                 pltpu.VMEM((chunks, rows, cw), BF16),
                 pltpu.VMEM((chunks, 3, own, cw), BF16),
-                dma((9,)), dma((3,)), dma((3,)),
-                dma((line + 1,)), dma((line + 1,)), dma((line + 1,)), dma((line + 1,)),
-                dma((2 * line,)), dma((2 * line,)),
+                dma((7,)), dma((9,)), dma((3,)), dma((3,)),
+                dma((2 * line + 2,)), dma((2 * line + 2,)), dma((2 * line + 2,)), dma((2 * line + 2,)),
+                dma((4 * line,)), dma((4 * line,)),
                 dma((1,)), dma((1,)),
                 dma((line + 1,)), dma((line + 1,)), dma((line + 1,)), dma((line + 1,)),
                 dma((3 * chunks,)), dma((3 * chunks,)),
             ],
             compiler_params=pltpu.CompilerParams(
-                collective_id=0, has_side_effects=True, vmem_limit_bytes=60 * 1024 * 1024
+                collective_id=0, has_side_effects=True, vmem_limit_bytes=56 * 1024 * 1024
             ),
         )(
             tokens, norm_gain.reshape(1, -1), mix_lambda.reshape(1, -1), attn_gain.reshape(1, -1),
-            gate_gap, extra_decay, init_state, rec_gain.reshape(1, -1),
+            gate_gap, extra_decay.transpose(0, 2, 1), init_state, rec_gain.reshape(1, -1),
             da_query, da_key, da_value, rec_query, rec_forget_fwd, rec_forget_bwd, rec_value,
             out_attn, out_rec,
         )

time: 45.7 us -> 43 us (0.941)
  local copies, waits for them, and re-layouts: 3.05 us -> 1.57 us
  Pallas kernels: 42.5 us -> 41.3 us
    unnamed x4 -> x1, local copies, waits for them, and re-layouts: 3.05 us -> 1.57 us
    pallas_call x1, Pallas kernels: 42.5 us -> 41.3 us  [local(): pl.pallas_call(functools.partial(kernel, line, tp_count, feats), out_shap...]
where the time goes in v2:
time: 43 us; the launch traced here: 42.9 us
  Pallas kernels  41.3 us (96%)
  local copies, waits for them, and re-layouts  1.57 us (4%)
    pallas_call x1, Pallas kernels, local(): pl.pallas_call(functools.partial(kernel, line, tp_count, feats), out_shap...  41.3 us
    unnamed x1, local copies, waits for them, and re-layouts  1.57 us

profile of v2, /device:TPU:0, one launch (start us, length us, event | category | flops | bytes accessed | tf_op | source)
XLA Modules:
  0.0 42.9 jit_solution(6653620057934997216)
XLA Ops:
  0.0 41.3 %shard_map.163 = bf16[32,2048]{1,0:T(8,128)(2,1)} custom-call(bf16[128,512]{1,0:T(8,128)(2,1)} %tokens.1, f32[1,2048]{1,0:T(1,128)} %bitcast.5, f32[1,2]{1,0:T(1,128)} %bitcast.7, f32[1,128]{1,0:T(1,128)} %bitcast.8, f32[2,256]{1,0:T(2,128)} %gap_h.1, f32[2,2,128]{2,1,0:T(2,128)} %bitcast.6, f32[2,2,128,128]{3,2,1,0:T(8,128)} %init_h.1, f32[1,128]{1,0:T(1,128)} %bitcast.9, ...), custom_call_target="tpu_custom_call" | custom-call | tf_op jit(solution)/shard_map/pallas_call | solution.py:399
  41.3 1.6 %copy.19 = bf16[32,2048]{1,0:T(8,128)(2,1)} copy(bf16[32,2048]{1,0:T(8,128)(2,1)} %shard_map.163) | data formatting | bytes 262144
